TPU v7x, 256 devices: a whole 4x4x8 slice. The times are simulated.
256 devices in a mesh: sp: 64 (over z, y, core), tp: 4 (over x).
Axes of the slice: x: 4, y: 4, z: 8, core: 2. Of those that a mesh axis runs over, the one named last changes fastest.
Arguments:
- query: bfloat16 [16384, 1024], P('sp', 'tp'), may hold values from -12 to 12
- key_rows: bfloat16 [16384, 512], P('sp', 'tp'), may hold values from -8 to 8
- value_rows: bfloat16 [16384, 512], P('sp', 'tp'), may hold values from -16 to 16
- stream: bfloat16 [16384, 2048], P(('sp', 'tp')), may hold values from -6 to 6
- out_weight: bfloat16 [1024, 2048], P('tp'), may hold values from -0.1875 to 0.1875
- norm_gain: float32 [2048], replicated, may hold values from 0.1 to 1.9
- route_ids: int32 [16384, 4], P(('sp', 'tp')), may hold values from 0 to 63, all different within a row; in each aligned block of 64 rows (0 to 63, 64 to 127, ...) at most 8 rows name the same one
- route_weights: float32 [16384, 4], P(('sp', 'tp')), may hold values from 0.1 to 1
- expert_gate: bfloat16 [64, 2048, 384], P('sp'), may hold values from -0.125 to 0.125
- expert_up: bfloat16 [64, 2048, 384], P('sp'), may hold values from -0.125 to 0.125
- expert_down: bfloat16 [64, 384, 2048], P('sp'), may hold values from -0.3125 to 0.3125
- shared_gate: bfloat16 [2048, 384], replicated, may hold values from -0.125 to 0.125
- shared_up: bfloat16 [2048, 384], replicated, may hold values from -0.125 to 0.125
- shared_down: bfloat16 [384, 2048], replicated, may hold values from -0.3125 to 0.3125
Outputs:
- result: bfloat16 [16384, 2048], P(('sp', 'tp'))
Inputs may be any that keep to these rules, and one draw needn't show every extreme that they name: `route_ids`: each row names 4 different experts. Within the rows of one device (aligned blocks of 64 rows) no expert is named more than 8 times, and in some blocks one expert is named exactly 8 times.
All inputs are finite; a program needn't handle non-finite values.
Results may differ from a plain program's by a relative error of at most 0.007.
Values may be sent and summed in bfloat16 or wider, within the bound.
No kernel may reach another device: no remote copies, remote signals or barrier semaphores. Data moves between devices by JAX's collectives and lax.ppermute only.
A program may use at most 128 MiB of HBM per device.

v0:
```python
import math

import jax
import jax.numpy as jnp
from jax import lax
from jax.sharding import Mesh
from jax.sharding import PartitionSpec as P

D = 2048
HD = 128
TOP_K = 4
KB = 128
SP = ("sp_0", "sp_1", "sp_2")
SP_TP = ("sp_0", "sp_1", "sp_2", "tp")


def joined_along(tiles, dim):
    tiles = jnp.moveaxis(tiles, 0, dim)
    shape = tiles.shape
    return tiles.reshape(*shape[:dim], shape[dim] * shape[dim + 1], *shape[dim + 2 :])


def all_blocks(value, axes, sequence):
    tiles = value[None]
    for k in sequence:
        tiles = lax.all_gather(tiles, axes[k], axis=0, tiled=True)
    block = [lax.axis_size(axes[k]) for k in reversed(sequence)]
    tiles = tiles.reshape(*block, *value.shape)
    turned = sorted(range(len(sequence)), key=lambda place: sequence[len(sequence) - 1 - place])
    return tiles.transpose(*turned, *range(len(sequence), tiles.ndim)).reshape(-1, *value.shape)


def gathered_by_axis(value, axes, sequence, dim):
    return joined_along(all_blocks(value, axes, sequence), dim)


def side_by_side(arrays, axis, dim, along):
    widths = [a.shape[along] for a in arrays]
    both = jnp.concatenate(arrays, axis=along)
    result = lax.all_gather(both, axis, axis=dim, tiled=True)
    return tuple(jnp.split(result, [sum(widths[:k]) for k in range(1, len(widths))], axis=along))


def soft_plus(values):
    return jnp.maximum(values, 0.0) + jnp.log1p(jnp.exp(-jnp.abs(values)))


def shard_scores(queries, shard_keys, shard_start, query_pos):
    key_count = shard_keys.shape[0]
    keys_split = shard_keys.reshape(key_count, queries.shape[1], queries.shape[3])
    logits = jnp.einsum("tkgd,skd->kgts", queries, keys_split, preferred_element_type=jnp.float32)
    logits = logits * (1.0 / math.sqrt(queries.shape[3]))
    key_pos = shard_start + jnp.arange(key_count, dtype=jnp.int32)
    visible = key_pos[None, :] < query_pos[:, None]
    penalty = soft_plus(logits)
    breaks = jnp.where(visible, -penalty, 0.0)
    return (logits, penalty, breaks, visible)


def grouped(values, block_size):
    full_shape = values.shape
    return values.reshape(full_shape[:-1] + (full_shape[-1] // block_size, block_size))


def later_matrix(length):
    positions = jnp.arange(length)
    return (positions[:, None] > positions[None, :]).astype(jnp.float32)


def later_sum(values, length):
    return jnp.einsum(
        "kgtm,mb->kgtb", values, later_matrix(length), precision=lax.Precision.HIGHEST
    )


def stick_weights(logits, penalty, breaks, visible, carried, block_size):
    inside = jnp.einsum(
        "kgtnj,js->kgtns",
        grouped(breaks, block_size),
        later_matrix(block_size),
        precision=lax.Precision.HIGHEST,
    )
    log_weight = (
        logits - penalty + inside.reshape(breaks.shape) + jnp.repeat(carried, block_size, axis=3)
    )
    return jnp.where(visible, jnp.exp(log_weight), 0.0).astype(jnp.bfloat16)


def add_values(running, weights, shard_values):
    values_split = shard_values.reshape(shard_values.shape[0], running.shape[0], running.shape[3])
    return running + jnp.einsum(
        "kgts,skd->kgtd", weights, values_split, preferred_element_type=jnp.float32
    )


def keep_state(current_state):
    return current_state


def per_device(
    query,
    key_rows,
    value_rows,
    stream,
    out_weight,
    norm_gain,
    route_ids,
    route_weights,
    expert_gate,
    expert_up,
    expert_down,
    shared_gate,
    shared_up,
    shared_down,
):
    tok_rows = query.shape[0]
    kv_local = key_rows.shape[1] // HD
    group_size = query.shape[1] // key_rows.shape[1]
    queries = query.reshape(tok_rows, kv_local, group_size, HD)
    device_pos = lax.axis_index(SP)
    offset = device_pos * tok_rows
    query_pos = offset + jnp.arange(tok_rows, dtype=jnp.int32)
    last_query = offset + tok_rows
    shard_blocks = tok_rows // KB
    total_blocks = lax.axis_size(SP) * shard_blocks
    zero_totals = jnp.zeros((kv_local, group_size, tok_rows, total_blocks), jnp.float32)
    zero_mixed = jnp.zeros((kv_local, group_size, tok_rows, HD), jnp.float32)
    key_piece = gathered_by_axis(key_rows, SP, (1, 0, 2), 0)
    key_shards = key_piece.reshape(-1, tok_rows, key_piece.shape[1])

    def visit_totals(current, scan_item):
        shard_keys, number = scan_item
        shard_start = number * tok_rows

        def evaluate_layer(current_state):
            breaks = shard_scores(queries, shard_keys, shard_start, query_pos)[2]
            first_block = shard_start // KB
            before = lax.dynamic_slice_in_dim(current_state, first_block, shard_blocks, 3)
            return lax.dynamic_update_slice_in_dim(
                current_state, before + grouped(breaks, KB).sum(axis=4), first_block, 3
            )

        return (lax.cond(shard_start < last_query, evaluate_layer, keep_state, current), None)

    numbers = jnp.arange(key_shards.shape[0], dtype=jnp.int32)
    totals = lax.scan(visit_totals, zero_totals, (key_shards, numbers))[0]
    across = later_sum(totals, total_blocks)
    pieces = side_by_side((key_rows, value_rows), SP, 0, 1)
    key_shards = pieces[0].reshape(-1, tok_rows, pieces[0].shape[1])
    value_shards = pieces[1].reshape(-1, tok_rows, pieces[1].shape[1])

    def visit_weighted(current, scan_item):
        shard_keys, shard_values, number = scan_item
        shard_start = number * tok_rows

        def evaluate_layer(current_state):
            logits, penalty, breaks, visible = shard_scores(
                queries, shard_keys, shard_start, query_pos
            )
            carried = lax.dynamic_slice_in_dim(across, shard_start // KB, shard_blocks, 3)
            weights = stick_weights(logits, penalty, breaks, visible, carried, KB)
            return add_values(current_state, weights, shard_values)

        return (lax.cond(shard_start < last_query, evaluate_layer, keep_state, current), None)

    numbers = jnp.arange(key_shards.shape[0], dtype=jnp.int32)
    mixed_sums = lax.scan(visit_weighted, zero_mixed, (key_shards, value_shards, numbers))[0]
    heads_out = (
        mixed_sums.astype(jnp.bfloat16)
        .transpose(2, 0, 1, 3)
        .reshape(tok_rows, kv_local * group_size * HD)
    )
    own_rows = stream.shape[0]
    token_heads = lax.all_to_all(heads_out, "tp", split_axis=0, concat_axis=1, tiled=True)
    attended = jnp.dot(
        token_heads,
        lax.all_gather(out_weight, "tp", axis=0, tiled=True),
        preferred_element_type=jnp.float32,
    )
    mid = (stream.astype(jnp.float32) + attended).astype(jnp.bfloat16)
    mid_wide = lax.optimization_barrier(mid).astype(jnp.float32)
    normed = (
        mid_wide
        * lax.rsqrt(jnp.mean(mid_wide * mid_wide, axis=1, keepdims=True) + 1e-06)
        * norm_gain
    ).astype(jnp.bfloat16)
    local_experts = expert_gate.shape[0]
    expert_count = lax.axis_size(SP) * local_experts
    capacity = 2 * own_rows * TOP_K // expert_count
    slot_count = expert_count * capacity
    flat_ids = route_ids.reshape(-1)
    membership = (flat_ids[:, None] == jnp.arange(expert_count, dtype=jnp.int32)[None, :]).astype(
        jnp.int32
    )
    before = jnp.cumsum(membership, axis=0) - membership
    slot_rank = jnp.sum(before * membership, axis=1)
    slot_ids = flat_ids * capacity + slot_rank
    placing = jnp.arange(slot_count, dtype=jnp.int32)[:, None] == slot_ids[None, :]
    dispatch = placing.reshape(slot_count, own_rows, TOP_K).any(axis=2).astype(jnp.bfloat16)
    outgoing = jnp.dot(dispatch, normed, preferred_element_type=jnp.float32).astype(jnp.bfloat16)
    outgoing = outgoing.reshape(lax.axis_size(SP), local_experts, capacity, D)
    arrived = lax.all_to_all(outgoing, SP, split_axis=0, concat_axis=0, tiled=True)
    gate_part = jnp.einsum(
        "sepd,edf->sepf", arrived, expert_gate, preferred_element_type=jnp.float32
    )
    up_part = jnp.einsum("sepd,edf->sepf", arrived, expert_up, preferred_element_type=jnp.float32)
    hidden = (jax.nn.silu(gate_part) * up_part).astype(jnp.bfloat16)
    produced = jnp.einsum(
        "sepf,efd->sepd", hidden, expert_down, preferred_element_type=jnp.float32
    ).astype(jnp.bfloat16)
    returned = lax.all_to_all(produced, SP, split_axis=0, concat_axis=0, tiled=True)
    returned = returned.reshape(slot_count, D)
    picking = (slot_ids[:, None] == jnp.arange(slot_count, dtype=jnp.int32)[None, :]).astype(
        jnp.bfloat16
    )
    selected_experts = jnp.dot(picking, returned, preferred_element_type=jnp.float32).reshape(
        own_rows, TOP_K, D
    )
    routed = jnp.sum(selected_experts * route_weights[:, :, None], axis=1)
    shared_hidden = (
        jax.nn.silu(jnp.dot(normed, shared_gate, preferred_element_type=jnp.float32))
        * jnp.dot(normed, shared_up, preferred_element_type=jnp.float32)
    ).astype(jnp.bfloat16)
    shared_out = jnp.dot(shared_hidden, shared_down, preferred_element_type=jnp.float32)
    return (mid_wide + routed + shared_out).astype(jnp.bfloat16)


def solution(mesh):
    split = Mesh(mesh.devices.reshape(8, 4, 2, mesh.shape["tp"]), ("sp_0", "sp_1", "sp_2", "tp"))
    in_specs = (
        P(SP, "tp"),
        P(SP, "tp"),
        P(SP, "tp"),
        P(SP_TP, None),
        P("tp", None),
        P(),
        P(SP_TP, None),
        P(SP_TP, None),
        P(SP, None, None),
        P(SP, None, None),
        P(SP, None, None),
        P(),
        P(),
        P(),
    )
    out_specs = P(SP_TP, None)
    return jax.shard_map(
        per_device, mesh=split, in_specs=in_specs, out_specs=out_specs, check_vma=False
    )
```

profile of v0, /device:TPU:8, one launch (start us, length us, event | category | flops | bytes accessed | tf_op | source)
XLA Modules:
  0.0 740.8 jit_solution(15018049518399371080)
XLA Ops:
  6.6 13.7 %all-gather = bf16[1024,128]{1,0:T(8,128)(2,1)} all-gather(bf16[256,128]{1,0:T(8,128)(2,1)} %param.23), channel_id=2, replica_groups=mesh['sp_0'=8,'sp_1'=4,'sp_2'=2,'tp'=4] {'sp_1'}, dimensions={0}, use_global_device_ids=true | all-gather | bytes 327680 | tf_op jit(solution)/shard_map/all_gather | solution.py:26
  20.4 43.3 %all-gather.8.cloned.1.call-done = bf16[32,256,128]{2,1,0:T(8,128)(2,1)} async-done(((bf16[4,256,128]{2,1,0:T(8,128)(2,1)}), bf16[32,256,128]{2,1,0:T(8,128)(2,1)}) %all-gather.8.cloned.1.call-update) | async-done | bytes 2097168 | tf_op jit(solution)/shard_map/all_gather | solution.py:26
  66.8 16.3 %all-gather.10.cloned.1.call-done = bf16[64,256,128]{2,1,0:T(8,128)(2,1)} async-done(((bf16[32,256,128]{2,1,0:T(8,128)(2,1)}), bf16[64,256,128]{2,1,0:T(8,128)(2,1)}) %all-gather.10.cloned.1.call-update) | async-done | bytes 4194320 | tf_op jit(solution)/shard_map/all_gather | solution.py:26
  83.1 4.6 copy.90
  87.7 88.4 %while.28 = (s32[]{:T(128)}, f32[1,2,256,128]{2,3,1,0:T(8,128)S(1)}, s32[64]{0:T(128)S(1)}, s32[]{:T(128)}, bf16[64,256,128]{2,1,0:T(8,128)(2,1)}, /*index=5*/bf...) while((s32[]{:T(128)}, f32[1,2,256,128]{2,3,1,0:T(8,128)S(1)}, ...), condition=%wide.region_4.5_spmd.clone, body=%wide.region_0.4_spmd.clone.sunk | while | flops 34669060 | bytes 1407887 | solution.py:146
  89.0 1.7 conditional.6
  89.1 1.3 bitcast_select_fusion
  92.0 1.7 conditional.6
  92.2 1.3 bitcast_select_fusion
  95.0 1.7 conditional.6
  95.2 1.3 bitcast_select_fusion
  176.5 5.9 fusion.97
  182.4 92.7 %while.29 = (s32[]{:T(128)}, f32[1,2,256,128]{3,2,1,0:T(8,128)S(1)}, s32[64]{0:T(128)S(1)}, s32[]{:T(128)}, bf16[64,256,128]{2,1,0:T(8,128)(2,1)}, /*index=5*/bf...) while((s32[]{:T(128)}, ...), condition=%wide.region_8.9_spmd.clone, body=%wide.region_5.8_spmd.clone.sunk | while | flops 270680576 | bytes 4672935 | solution.py:167
  183.7 3.4 conditional.7
  183.9 1.3 negate_select_fusion
  186.0 1.1 fusion.9
  188.4 3.4 conditional.7
  188.6 1.3 negate_select_fusion
  193.1 3.4 conditional.7
  193.3 1.3 negate_select_fusion
  195.4 1.1 fusion.9
  276.1 4.3 all-to-all-start
  280.5 5.8 all-to-all-done
  286.4 3.0 fusion.26
  290.4 371.3 %all_to_all.29 = bf16[64,1,8,2048]{3,2,1,0:T(8,128)(2,1)S(1)} all-to-all(bf16[64,1,8,2048]{3,2,1,0:T(8,128)(2,1)S(1)} %fusion.24), channel_id=1, replica_groups=mesh['sp_0'=8,'sp_1'=4,'sp_2'=2,'tp'=4] {'sp_0','sp_1','sp_2'}, dimensions={0} | all-to-all | bytes 4194304 | tf_op jit(solution)/shard_map/all_to_all | solution.py:202
  661.7 1.3 copy-done.1
  663.0 2.2 fusion.39
  665.2 5.9 fusion.25
  671.1 5.8 all-to-all-start.2
  677.3 50.7 %all-to-all-done.2 = bf16[64,1,8,2048]{3,2,1,0:T(8,128)(2,1)} async-done(((bf16[64,1,8,2048]{3,2,1,0:T(8,128)(2,1)}), bf16[64,1,8,2048]{3,2,1,0:T(8,128)(2,1)}, u32[]{:S(2)}, u32[]{:S(2)}) %all-to-all-start.2) | async-done | bytes 2097184 | tf_op jit(solution)/shard_map/all_to_all | solution.py:211
  728.0 3.2 fusion.36
  731.2 3.1 fusion.27
  (471 shorter events, 89.0 us)
Async XLA Ops:
  6.5 658.7 %copy-start = (bf16[1,384,2048]{2,1,0:T(8,128)(2,1)S(1)}, bf16[1,384,2048]{2,1,0:T(8,128)(2,1)}, u32[]{:S(2)}) copy-start(bf16[1,384,2048]{2,1,0:T(8,128)(2,1)} %param.32) | copy-start | bytes 4718596
  6.5 57.2 %copy-start.5 = (bf16[256,128]{1,0:T(8,128)(2,1)S(1)}, bf16[256,128]{1,0:T(8,128)(2,1)}, u32[]{:S(2)}) copy-start(bf16[256,128]{1,0:T(8,128)(2,1)} %param.23) | copy-start | bytes 196612
  6.5 57.2 %copy-start.8 = (bf16[256,128]{1,0:T(8,128)(2,1)S(1)}, bf16[256,128]{1,0:T(8,128)(2,1)}, u32[]{:S(2)}) copy-start(bf16[256,128]{1,0:T(8,128)(2,1)} %param.24) | copy-start | bytes 196612
  6.5 58.5 %copy-start.9 = (s32[64,4]{0,1:T(4,128)S(1)}, s32[64,4]{0,1:T(4,128)}, u32[]{:S(2)}) copy-start(s32[64,4]{0,1:T(4,128)} %param.28) | copy-start | bytes 3076
  6.5 58.8 %copy-start.6 = (bf16[256,256]{1,0:T(8,128)(2,1)S(1)}, bf16[256,256]{1,0:T(8,128)(2,1)}, u32[]{:S(2)}) copy-start(bf16[256,256]{1,0:T(8,128)(2,1)} %param.22) | copy-start | bytes 393220
  6.5 57.1 %all-gather.8.cloned.1.call-start = ((), (), s32[]{:S(2)}) async-start(), calls=%async_computation.4 | async-start | bytes 2359296 | tf_op jit(solution)/shard_map/all_gather | solution.py:26
  20.3 62.7 %all-gather.10.cloned.1.call-start = ((), (), s32[]{:S(2)}) async-start(), calls=%async_computation.5 | async-start | bytes 6291456 | tf_op jit(solution)/shard_map/all_gather | solution.py:26
  63.7 112.8 %all-gather.6.cloned.1.call-start = ((), (), s32[]{:S(2)}) async-start(), calls=%async_computation.3 | async-start | bytes 8519680 | tf_op jit(solution)/shard_map/all_gather | solution.py:40
  64.5 221.9 %all-gather.12.cloned.1.call-start = ((), (), s32[]{:S(2)}) async-start(), calls=%async_computation.6 | async-start | bytes 5242880 | tf_op jit(solution)/shard_map/all_gather | solution.py:177
  182.4 103.9 %copy-start.4 = (bf16[64,2048]{1,0:T(8,128)(2,1)S(1)}, bf16[64,2048]{1,0:T(8,128)(2,1)}, u32[]{:S(2)}) copy-start(bf16[64,2048]{1,0:T(8,128)(2,1)} %param.25) | copy-start | bytes 786436
  276.1 10.2 %all-to-all-start = ((bf16[4,64,256]{2,1,0:T(8,128)(2,1)}), bf16[4,64,256]{2,1,0:T(8,128)(2,1)S(1)}, u32[]{:S(2)}, u32[]{:S(2)}) async-start(bf16[4,64,256]{2,1,0:T(8,128)(2,1)} %all_to_all.20), calls=%async_computation | async-start | bytes 262144 | tf_op jit(solution)/shard_map/all_to_all | solution.py:174
  286.4 3.2 copy-start.7
  290.4 372.7 %copy-start.10 = (bf16[1,2048,384]{2,1,0:T(8,128)(2,1)S(1)}, bf16[1,2048,384]{2,1,0:T(8,128)(2,1)}, u32[]{:S(2)}) copy-start(bf16[1,2048,384]{2,1,0:T(8,128)(2,1)} %param.30) | copy-start | bytes 4718596
  661.7 1.3 copy-start.1
  671.1 5.8 copy-start.3
  671.1 56.9 %copy-start.11 = (f32[64,4]{0,1:T(4,128)S(1)}, f32[64,4]{0,1:T(4,128)}, u32[]{:S(2)}) copy-start(f32[64,4]{0,1:T(4,128)} %param.29) | copy-start | bytes 3076
  671.1 56.9 %all-to-all-start.2 = ((bf16[64,1,8,2048]{3,2,1,0:T(8,128)(2,1)}), bf16[64,1,8,2048]{3,2,1,0:T(8,128)(2,1)}, u32[]{:S(2)}, u32[]{:S(2)}) async-start(bf16[64,1,8,2048]{3,2,1,0:T(8,128)(2,1)} %fusion.25), calls=%async_computation.2 | async-start | bytes 4194304 | tf_op jit(solution)/shard_map/all_to_all | solution.py:211
  677.3 53.9 %copy-start.2 = (bf16[384,2048]{1,0:T(8,128)(2,1)S(1)}, bf16[384,2048]{1,0:T(8,128)(2,1)}, u32[]{:S(2)}) copy-start(bf16[384,2048]{1,0:T(8,128)(2,1)} %param.35) | copy-start | bytes 4718596
Sparse Core Ops, SparseCore 0:
  20.5 43.1 all-gather.7
  65.5 17.5 all-gather.9
  85.8 83.1 all-gather.5
  170.7 48.8 all-gather.11
where the time goes:
time: 751 us; the launch traced here: 741 us
  blocking collectives  385 us (51%)
  waiting for transfers between devices  117 us (16%)
  local copies, waits for them, and re-layouts  91.1 us (12%)
  loops' own time  89.3 us (12%)
  matrix products  31.4 us (4%)
  between operations  13.4 us (2%)
  starting transfers between devices  10.2 us (1%)
    all_to_all x1, blocking collectives, per_device(): lax.all_to_all(outgoing, SP, split_axis=0, concat_axis=0, tiled=True)  371 us
    dynamic_slice x128, local copies, waits for them, and re-layouts, per_device(): totals = lax.scan(visit_totals, zero_totals, (key_shards, numbers))[0]  76.5 us
    all_gather x2, waiting for transfers between devices, all_blocks(): tiles = lax.all_gather(tiles, axes[k], axis=0, tiled=True)  59.6 us
    all_to_all x1, waiting for transfers between devices, per_device(): lax.all_to_all(produced, SP, split_axis=0, concat_axis=0, tiled=True)  50.7 us
    another operation x1, loops' own time, per_device(): lax.scan(visit_weighted, zero_mixed, (key_shards, value_shards, numbers))[0]  44.1 us
    another operation x1, loops' own time, per_device(): totals = lax.scan(visit_totals, zero_totals, (key_shards, numbers))[0]  43.3 us
  transfers between devices with their start and end apart: 6, of which 4 were waited for; matrix products, arithmetic and copies ran while one was open for 14% of the time, Pallas kernels for 0%

commit v1 on v0

v1 whole, which is shorter than its diff:
```python
import math

import jax
import jax.numpy as jnp
from jax import lax
from jax.experimental import pallas as pl
from jax.experimental.pallas import tpu as pltpu
from jax.sharding import Mesh
from jax.sharding import PartitionSpec as P

D = 2048
HD = 128
TOP_K = 4
KB = 128
SP = ("sp_0", "sp_1", "sp_2")
SP_TP = ("sp_0", "sp_1", "sp_2", "tp")


BK = 256
SCALE = math.log2(math.e) / math.sqrt(HD)


def attention_kernel(pos_ref, q_ref, kv_ref, o_ref, q2, acc, carry, tri, dbuf, sbuf):
    tok = q_ref.shape[0]
    heads = q_ref.shape[1] // HD
    rows = tok * heads
    for g in range(heads):
        scaled = q_ref[:, g * HD : (g + 1) * HD].astype(jnp.float32) * SCALE
        high = scaled.astype(jnp.bfloat16)
        q2[pl.ds(g * tok, tok), 0:HD] = high
        q2[pl.ds(g * tok, tok), HD : 2 * HD] = (scaled - high.astype(jnp.float32)).astype(
            jnp.bfloat16
        )
    acc[...] = jnp.zeros_like(acc)
    carry[...] = jnp.zeros_like(carry)
    key_at = lax.broadcasted_iota(jnp.int32, (BK, BK), 0)
    tri[...] = (
        (key_at > lax.broadcasted_iota(jnp.int32, (BK, BK), 1))
        .astype(jnp.float32)
        .astype(jnp.bfloat16)
    )
    pos = pos_ref[0]

    def scores(j, slot, diagonal):
        start = pl.multiple_of(j * BK, BK)
        keys = kv_ref[pl.ds(start, BK), 0:HD]
        y = lax.dot_general(
            q2[...],
            jnp.concatenate([keys, keys], axis=1),
            (((1,), (1,)), ((), ())),
            preferred_element_type=jnp.float32,
        )
        penalty = jnp.maximum(y, jnp.log2(1.0 + jnp.exp2(jnp.minimum(y, 126.0))))
        level = y - penalty
        if diagonal:
            query_at = lax.broadcasted_iota(jnp.int32, (rows, BK), 0) % tok
            visible = lax.broadcasted_iota(jnp.int32, (rows, BK), 1) < query_at
            penalty = jnp.where(visible, penalty, 0.0)
            level = jnp.where(visible, level, -1e30)
        dbuf[slot] = level
        sbuf[slot] = penalty.astype(jnp.bfloat16)

    def mix(j, slot):
        start = pl.multiple_of(j * BK, BK)
        values = kv_ref[pl.ds(start, BK), HD : 2 * HD]
        penalty = sbuf[slot]
        after = jnp.dot(penalty, tri[...], preferred_element_type=jnp.float32)
        so_far = carry[...]
        weights = jnp.exp2(dbuf[slot] - after - jnp.concatenate([so_far, so_far], axis=1))
        carry[...] = so_far + jnp.broadcast_to(
            after[:, 0:1] + penalty[:, 0:1].astype(jnp.float32), (rows, HD)
        )
        acc[...] += jnp.dot(
            weights.astype(jnp.bfloat16), values, preferred_element_type=jnp.float32
        )

    def both(j, slot):
        mix(j, slot)
        scores(j - 1, 1 - slot, False)

    scores(pos, 0, True)

    def step(i, _):
        both(pos - 2 * i, 0)
        both(pos - 2 * i - 1, 1)
        return 0

    lax.fori_loop(0, pos // 2, step, 0)

    @pl.when(pos % 2 == 1)
    def _():
        both(1, 0)
        mix(0, 1)

    @pl.when(pos % 2 == 0)
    def _():
        mix(0, 0)

    for g in range(heads):
        o_ref[:, g * HD : (g + 1) * HD] = acc[pl.ds(g * tok, tok), :].astype(o_ref.dtype)


def attention(query, pairs, device_pos):
    tok = query.shape[0]
    rows = tok * (query.shape[1] // HD)
    steps = pairs.shape[0] // BK
    return pl.pallas_call(
        attention_kernel,
        out_shape=jax.ShapeDtypeStruct(query.shape, jnp.bfloat16),
        in_specs=[
            pl.BlockSpec(memory_space=pltpu.SMEM),
            pl.BlockSpec(memory_space=pltpu.VMEM),
            pl.BlockSpec(memory_space=pltpu.VMEM),
        ],
        out_specs=pl.BlockSpec(memory_space=pltpu.VMEM),
        scratch_shapes=[
            pltpu.VMEM((rows, 2 * HD), jnp.bfloat16),
            pltpu.VMEM((rows, HD), jnp.float32),
            pltpu.VMEM((rows, HD), jnp.float32),
            pltpu.VMEM((BK, BK), jnp.bfloat16),
            pltpu.VMEM((2, rows, BK), jnp.float32),
            pltpu.VMEM((2, rows, BK), jnp.bfloat16),
        ],
        compiler_params=pltpu.CompilerParams(vmem_limit_bytes=40 * 2**20),
        cost_estimate=pl.CostEstimate(
            flops=steps * rows * BK * HD * 8, bytes_accessed=pairs.size * 2, transcendentals=0
        ),
        name="stick",
    )(device_pos.reshape(1), query, pairs)


def per_device(
    query,
    key_rows,
    value_rows,
    stream,
    out_weight,
    norm_gain,
    route_ids,
    route_weights,
    expert_gate,
    expert_up,
    expert_down,
    shared_gate,
    shared_up,
    shared_down,
):
    device_pos = lax.axis_index(SP)
    pairs = lax.all_gather(
        jnp.concatenate([key_rows, value_rows], axis=1), SP, axis=0, tiled=True
    )
    heads_out = attention(query, pairs, device_pos)
    own_rows = stream.shape[0]
    token_heads = lax.all_to_all(heads_out, "tp", split_axis=0, concat_axis=1, tiled=True)
    attended = jnp.dot(
        token_heads,
        lax.all_gather(out_weight, "tp", axis=0, tiled=True),
        preferred_element_type=jnp.float32,
    )
    mid = (stream.astype(jnp.float32) + attended).astype(jnp.bfloat16)
    mid_wide = lax.optimization_barrier(mid).astype(jnp.float32)
    normed = (
        mid_wide
        * lax.rsqrt(jnp.mean(mid_wide * mid_wide, axis=1, keepdims=True) + 1e-06)
        * norm_gain
    ).astype(jnp.bfloat16)
    local_experts = expert_gate.shape[0]
    expert_count = lax.axis_size(SP) * local_experts
    capacity = 2 * own_rows * TOP_K // expert_count
    slot_count = expert_count * capacity
    flat_ids = route_ids.reshape(-1)
    membership = (flat_ids[:, None] == jnp.arange(expert_count, dtype=jnp.int32)[None, :]).astype(
        jnp.int32
    )
    before = jnp.cumsum(membership, axis=0) - membership
    slot_rank = jnp.sum(before * membership, axis=1)
    slot_ids = flat_ids * capacity + slot_rank
    placing = jnp.arange(slot_count, dtype=jnp.int32)[:, None] == slot_ids[None, :]
    dispatch = placing.reshape(slot_count, own_rows, TOP_K).any(axis=2).astype(jnp.bfloat16)
    outgoing = jnp.dot(dispatch, normed, preferred_element_type=jnp.float32).astype(jnp.bfloat16)
    outgoing = outgoing.reshape(lax.axis_size(SP), local_experts, capacity, D)
    arrived = lax.all_to_all(outgoing, SP, split_axis=0, concat_axis=0, tiled=True)
    gate_part = jnp.einsum(
        "sepd,edf->sepf", arrived, expert_gate, preferred_element_type=jnp.float32
    )
    up_part = jnp.einsum("sepd,edf->sepf", arrived, expert_up, preferred_element_type=jnp.float32)
    hidden = (jax.nn.silu(gate_part) * up_part).astype(jnp.bfloat16)
    produced = jnp.einsum(
        "sepf,efd->sepd", hidden, expert_down, preferred_element_type=jnp.float32
    ).astype(jnp.bfloat16)
    returned = lax.all_to_all(produced, SP, split_axis=0, concat_axis=0, tiled=True)
    returned = returned.reshape(slot_count, D)
    picking = (slot_ids[:, None] == jnp.arange(slot_count, dtype=jnp.int32)[None, :]).astype(
        jnp.bfloat16
    )
    selected_experts = jnp.dot(picking, returned, preferred_element_type=jnp.float32).reshape(
        own_rows, TOP_K, D
    )
    routed = jnp.sum(selected_experts * route_weights[:, :, None], axis=1)
    shared_hidden = (
        jax.nn.silu(jnp.dot(normed, shared_gate, preferred_element_type=jnp.float32))
        * jnp.dot(normed, shared_up, preferred_element_type=jnp.float32)
    ).astype(jnp.bfloat16)
    shared_out = jnp.dot(shared_hidden, shared_down, preferred_element_type=jnp.float32)
    return (mid_wide + routed + shared_out).astype(jnp.bfloat16)


def solution(mesh):
    split = Mesh(mesh.devices.reshape(8, 4, 2, mesh.shape["tp"]), ("sp_0", "sp_1", "sp_2", "tp"))
    in_specs = (
        P(SP, "tp"),
        P(SP, "tp"),
        P(SP, "tp"),
        P(SP_TP, None),
        P("tp", None),
        P(),
        P(SP_TP, None),
        P(SP_TP, None),
        P(SP, None, None),
        P(SP, None, None),
        P(SP, None, None),
        P(),
        P(),
        P(),
    )
    out_specs = P(SP_TP, None)
    return jax.shard_map(
        per_device, mesh=split, in_specs=in_specs, out_specs=out_specs, check_vma=False
    )
```

time: 751 us -> 292 us (0.39); the launches traced: 741 us -> 292 us
  blocking collectives: 385 us -> 63 us
  loops' own time: 89.3 us -> 0 us
  local copies, waits for them, and re-layouts: 91.1 us -> 6.97 us
  waiting for transfers between devices: 117 us -> 174 us
  matrix products: 31.4 us -> 18.6 us
    all_to_all x1, blocking collectives: 371 us -> 63 us  [per_device(): lax.all_to_all(outgoing, SP, split_axis=0, concat_axis=0, tiled=True)]
    another operation x130 -> x0, loops' own time: 89.3 us -> none  [the longest x1 44.1 us: per_device(): lax.scan(visit_weighted, zero_mixed, (key_shards, value_shards, numbers))[0]]
    dynamic_slice x131 -> x0, local copies, waits for them, and re-layouts: 76.5 us -> none  [the longest x128 76.5 us: per_device(): totals = lax.scan(visit_totals, zero_totals, (key_shards, numbers))[0]]
    all_gather x1, waiting for transfers between devices: 0.02 us -> 34.1 us  [per_device(): lax.all_gather(out_weight, 'tp', axis=0, tiled=True)]
    all_gather x3 -> x1, waiting for transfers between devices: 59.6 us -> 82.9 us  [per_device(): lax.all_gather(jnp.concatenate([key_rows, value_rows], axis=1), SP, axis=...]
    all_gather x1 -> x0, blocking collectives: 13.7 us -> none  [all_blocks(): tiles = lax.all_gather(tiles, axes[k], axis=0, tiled=True)]
    dot_general x13 -> x0, matrix products: 12.8 us -> none  [the longest x6 7.93 us: shard_scores(): jnp.einsum('tkgd,skd->kgts', queries, keys_split, preferred_element_type=...]
  transfers between devices with their start and end apart: 6 -> 4, of which waited for: 4 -> 4; matrix products, arithmetic and copies ran while one was open for 14% -> 1% of each run, Pallas kernels for 0% -> 1%
where the time goes in v1:
time: 292 us
  waiting for transfers between devices  174 us (60%)
  blocking collectives  63 us (22%)
  matrix products  18.6 us (6%)
  between operations  13.5 us (5%)
  starting transfers between devices  10 us (3%)
  local copies, waits for them, and re-layouts  6.97 us (2%)
  other arithmetic  3.42 us (1%)
    all_gather x1, waiting for transfers between devices, per_device(): lax.all_gather(jnp.concatenate([key_rows, value_rows], axis=1), SP, axis=...  82.9 us
    all_to_all x1, blocking collectives, per_device(): lax.all_to_all(outgoing, SP, split_axis=0, concat_axis=0, tiled=True)  63 us
    all_to_all x1, waiting for transfers between devices, per_device(): lax.all_to_all(produced, SP, split_axis=0, concat_axis=0, tiled=True)  50.7 us
    all_gather x1, waiting for transfers between devices, per_device(): lax.all_gather(out_weight, 'tp', axis=0, tiled=True)  34.1 us
    unnamed x21, local copies, waits for them, and re-layouts  6.38 us
    dot_general x1, matrix products, per_device(): jnp.einsum('sepf,efd->sepd', hidden, expert_down, preferred_element_type=...  5.92 us
    all_to_all x1, waiting for transfers between devices, per_device(): lax.all_to_all(heads_out, 'tp', split_axis=0, concat_axis=1, tiled=True)  5.89 us
  transfers between devices with their start and end apart: 4, of which 4 were waited for; matrix products, arithmetic and copies ran while one was open for 1% of the time, Pallas kernels for 1%

profile of v1, /device:TPU:8, one launch (start us, length us, event | category | flops | bytes accessed | tf_op | source)
XLA Modules:
  0.0 291.9 jit_solution(8953474209960735643)
XLA Ops:
  6.5 1.7 pad_maximum_fusion
  8.2 0.0 all-gather.5.cloned.1.call-start
  8.3 0.7 all-gather.5.cloned.1.call-update
  9.0 0.8 copy.43
  9.8 0.1 eq.72
  9.9 0.1 eq.68
  10.0 0.6 reduce-window.6
  10.6 0.2 slice_reduce_fusion
  10.8 0.1 fusion.60
  10.9 0.1 reduce_sum.30
  11.1 0.1 copy.46
  11.1 0.7 multiply_add_fusion
  11.8 82.9 %all-gather.3.cloned.1.call-done.kv_ref = bf16[16384,256]{1,0:T(8,128)(2,1)} async-done(((bf16[256,256]{1,0:T(8,128)(2,1)}), bf16[16384,256]{1,0:T(8,128)(2,1)}) %all-gather.3.cloned.1.call-update) | async-done | bytes 8388624 | tf_op jit(solution)/shard_map/all_gather | solution.py:149
  94.7 3.4 %copy-done.1 = bf16[16384,256]{1,0:T(8,128)(2,1)S(1)} copy-done((bf16[16384,256]{1,0:T(8,128)(2,1)S(1)}, bf16[16384,256]{1,0:T(8,128)(2,1)}, u32[]{:S(2)}) %copy-start.1) | copy-done | bytes 8388632
  98.1 0.9 copy-done.2
  99.0 2.1 stick.1
  101.2 4.2 %all-to-all-start = ((bf16[4,64,256]{2,1,0:T(8,128)(2,1)}), bf16[4,64,256]{2,1,0:T(8,128)(2,1)S(1)}, u32[]{:S(2)}, u32[]{:S(2)}) async-start(bf16[4,64,256]{2,1,0:T(8,128)(2,1)} %bitcast.1), calls=%async_computation | async-start | bytes 262144 | tf_op jit(solution)/shard_map/all_to_all | solution.py:154
  105.4 0.1 fusion.50
  105.6 5.9 %all-to-all-done = bf16[4,64,256]{2,1,0:T(8,128)(2,1)S(1)} async-done(((bf16[4,64,256]{2,1,0:T(8,128)(2,1)}), bf16[4,64,256]{2,1,0:T(8,128)(2,1)S(1)}, u32[]{:S(2)}, u32[]{:S(2)}) %all-to-all-start) | async-done | bytes 131104 | tf_op jit(solution)/shard_map/all_to_all | solution.py:154
  111.5 34.1 %all-gather.5.cloned.1.call-done = bf16[1024,2048]{1,0:T(8,128)(2,1)} async-done(((bf16[256,2048]{1,0:T(8,128)(2,1)}), bf16[1024,2048]{1,0:T(8,128)(2,1)}) %all-gather.5.cloned.1.call-update) | async-done | bytes 4194320 | tf_op jit(solution)/shard_map/all_gather | solution.py:157
  145.5 3.0 %fusion.2 = bf16[64,2048]{1,0:T(8,128)(2,1)S(1)} fusion(bf16[64,1024]{1,0:T(8,128)(2,1)S(1)} %bitcast.117, bf16[1024,2048]{1,0:T(8,128)(2,1)} %all-gather.5.cloned.1.call-done, bf16[64,2048]{1,0:T(8,128)(2,1)S(1)} %copy-done.6), kind=kOutput, calls=%fused_computation.7 | convolution fusion | flops 268828672 | bytes 4849664 | tf_op jit(solution)/shard_map/dot_general | solution.py:155
  148.6 0.2 fusion.45
  148.7 0.8 fusion
  149.5 63.0 %all_to_all.29 = bf16[64,1,8,2048]{3,2,1,0:T(8,128)(2,1)S(1)} all-to-all(bf16[64,1,8,2048]{3,2,1,0:T(8,128)(2,1)S(1)} %fusion), channel_id=1, replica_groups=mesh['sp_0'=8,'sp_1'=4,'sp_2'=2,'tp'=4] {'sp_0','sp_1','sp_2'}, dimensions={0} | all-to-all | bytes 4194304 | tf_op jit(solution)/shard_map/all_to_all | solution.py:182
  212.5 1.3 copy-done.3
  213.8 2.1 fusion.15
  216.0 5.9 %fusion.1 = bf16[64,1,8,2048]{3,2,1,0:T(8,128)(2,1)} fusion(bf16[1,384,2048]{2,1,0:T(8,128)(2,1)S(1)} %copy-done, bf16[1,2048,384]{2,1,0:T(8,128)(2,1)} %param.23, bf16[64,1,8,2048]{3,2,1,0:T(8,128)(2,1)} %copy-done.3, f32[64,1,8,384]{3,2,0,1:T(8,128)} %fusion.15), kind=kOutput, calls=%fused_computation.3 | convolution fusion | flops 1612840960 | bytes 8126464 | tf_op jit(solution)/shard_map/sepf,efd->sepd/dot_general | solution.py:188
  221.9 5.8 %all-to-all-start.2 = ((bf16[64,1,8,2048]{3,2,1,0:T(8,128)(2,1)}), bf16[64,1,8,2048]{3,2,1,0:T(8,128)(2,1)}, u32[]{:S(2)}, u32[]{:S(2)}) async-start(bf16[64,1,8,2048]{3,2,1,0:T(8,128)(2,1)} %fusion.1), calls=%async_computation.2 | async-start | bytes 4194304 | tf_op jit(solution)/shard_map/all_to_all | solution.py:191
  227.7 0.4 fusion.65
  228.1 50.7 %all-to-all-done.2 = bf16[64,1,8,2048]{3,2,1,0:T(8,128)(2,1)} async-done(((bf16[64,1,8,2048]{3,2,1,0:T(8,128)(2,1)}), bf16[64,1,8,2048]{3,2,1,0:T(8,128)(2,1)}, u32[]{:S(2)}, u32[]{:S(2)}) %all-to-all-start.2) | async-done | bytes 2097184 | tf_op jit(solution)/shard_map/all_to_all | solution.py:191
  278.8 3.2 %fusion.12 = f32[64,2048]{1,0:T(8,128)} fusion(bf16[64,1,8,2048]{3,2,1,0:T(8,128)(2,1)} %all-to-all-done.2, f32[64,4]{0,1:T(4,128)S(1)} %copy-done.9, s32[64,4]{0,1:T(4,128)S(1)} %multiply_add_fusion), kind=kOutput, calls=%fused_computation.17 | convolution fusion | flops 537919488 | bytes 2623488 | tf_op jit(solution)/shard_map/dot_general | solution.py:196
  282.0 3.1 %fusion.3 = bf16[64,2048]{1,0:T(8,128)(2,1)} fusion(bf16[384,2048]{1,0:T(8,128)(2,1)S(1)} %copy-done.4, bf16[2048,384]{1,0:T(8,128)(2,1)} %param.26, f32[64,2048]{1,0:T(8,128)} %fusion.12, bf16[64,2048]{1,0:T(8,128)(2,1)S(1)} %fusion.2, f32[64,384]{1,0:T(8,128)S(1)} %fusion.65, f32[2048]{0:T(1024)S(1)} %copy-done.7, f32[64]{0:T(128)S(1)} %add_rsqrt_fusion), kind=kOutput, calls=%fused_computation.8 | convolution fusion | flops 202522624 | bytes 4301056 | tf_op jit(solution)/shard_map/dot_general | solution.py:204
  (24 shorter events, 0.1 us)
Async XLA Ops:
  6.5 209.4 %copy-start = (bf16[1,384,2048]{2,1,0:T(8,128)(2,1)S(1)}, bf16[1,384,2048]{2,1,0:T(8,128)(2,1)}, u32[]{:S(2)}) copy-start(bf16[1,384,2048]{2,1,0:T(8,128)(2,1)} %param.24) | copy-start | bytes 4718596
  6.5 88.2 %all-gather.3.cloned.1.call-start = ((), (), s32[]{:S(2)}) async-start(), calls=%async_computation.3 | async-start | bytes 8519680 | tf_op jit(solution)/shard_map/all_gather | solution.py:149
  8.2 137.3 %all-gather.5.cloned.1.call-start = ((), (), s32[]{:S(2)}) async-start(), calls=%async_computation.4 | async-start | bytes 5242880 | tf_op jit(solution)/shard_map/all_gather | solution.py:157
  94.7 3.4 %copy-start.1 = (bf16[16384,256]{1,0:T(8,128)(2,1)S(1)}, bf16[16384,256]{1,0:T(8,128)(2,1)}, u32[]{:S(2)}) copy-start(bf16[16384,256]{1,0:T(8,128)(2,1)} %all-gather.3.cloned.1.call-done.kv_ref) | copy-start | bytes 25165828
  98.1 0.9 copy-start.2
  99.0 46.5 %copy-start.6 = (bf16[64,2048]{1,0:T(8,128)(2,1)S(1)}, bf16[64,2048]{1,0:T(8,128)(2,1)}, u32[]{:S(2)}) copy-start(bf16[64,2048]{1,0:T(8,128)(2,1)} %param.17) | copy-start | bytes 786436
  101.2 10.3 %all-to-all-start = ((bf16[4,64,256]{2,1,0:T(8,128)(2,1)}), bf16[4,64,256]{2,1,0:T(8,128)(2,1)S(1)}, u32[]{:S(2)}, u32[]{:S(2)}) async-start(bf16[4,64,256]{2,1,0:T(8,128)(2,1)} %bitcast.1), calls=%async_computation | async-start | bytes 262144 | tf_op jit(solution)/shard_map/all_to_all | solution.py:154
  145.5 3.2 %copy-start.7 = (f32[2048]{0:T(1024)S(1)}, f32[2048]{0:T(1024)}, u32[]{:S(2)}) copy-start(f32[2048]{0:T(1024)} %param.19) | copy-start | bytes 24580
  149.5 64.3 %copy-start.8 = (bf16[1,2048,384]{2,1,0:T(8,128)(2,1)S(1)}, bf16[1,2048,384]{2,1,0:T(8,128)(2,1)}, u32[]{:S(2)}) copy-start(bf16[1,2048,384]{2,1,0:T(8,128)(2,1)} %param.22) | copy-start | bytes 4718596
  212.5 1.3 copy-start.3
  221.9 5.8 %copy-start.5 = (bf16[2048,384]{1,0:T(8,128)(2,1)S(1)}, bf16[2048,384]{1,0:T(8,128)(2,1)}, u32[]{:S(2)}) copy-start(bf16[2048,384]{1,0:T(8,128)(2,1)} %param.25) | copy-start | bytes 4718596
  221.9 56.9 %copy-start.9 = (f32[64,4]{0,1:T(4,128)S(1)}, f32[64,4]{0,1:T(4,128)}, u32[]{:S(2)}) copy-start(f32[64,4]{0,1:T(4,128)} %param.21) | copy-start | bytes 3076
  221.9 56.9 %all-to-all-start.2 = ((bf16[64,1,8,2048]{3,2,1,0:T(8,128)(2,1)}), bf16[64,1,8,2048]{3,2,1,0:T(8,128)(2,1)}, u32[]{:S(2)}, u32[]{:S(2)}) async-start(bf16[64,1,8,2048]{3,2,1,0:T(8,128)(2,1)} %fusion.1), calls=%async_computation.2 | async-start | bytes 4194304 | tf_op jit(solution)/shard_map/all_to_all | solution.py:191
  228.1 53.9 %copy-start.4 = (bf16[384,2048]{1,0:T(8,128)(2,1)S(1)}, bf16[384,2048]{1,0:T(8,128)(2,1)}, u32[]{:S(2)}) copy-start(bf16[384,2048]{1,0:T(8,128)(2,1)} %param.27) | copy-start | bytes 4718596
Sparse Core Ops, SparseCore 0:
  10.1 84.5 all-gather.2
  96.5 48.9 all-gather.4
